TPU v7x, 32 devices: a whole 2x2x4 slice. The times are simulated.
32 devices in a mesh: ep: 8 (over z, x), tp: 4 (over y, core).
Axes of the slice: x: 2, y: 2, z: 4, core: 2. Of those that a mesh axis runs over, the one named last changes fastest.
Arguments:
- tokens: bfloat16 [1024, 2048], P('ep'), may hold values from -6 to 6
- chosen: int32 [8, 8, 7], P('ep'), may hold values from -1 to 127, as said below
- pick_weight: float32 [8, 8, 7], P('ep'), may hold values from 0.2 to 1
- gate_weight: bfloat16 [8, 2048, 4096], P('ep', None, 'tp'), may hold values from -0.125 to 0.125
- up_weight: bfloat16 [8, 2048, 4096], P('ep', None, 'tp'), may hold values from -0.125 to 0.125
- down_weight: bfloat16 [8, 4096, 2048], P('ep', 'tp'), may hold values from -0.09375 to 0.09375
Outputs:
- combined: bfloat16 [1024, 2048], P('ep', 'tp')
Inputs may be any that keep to these rules, and one draw needn't show every extreme that they name: `chosen`: within one group and one expert the named positions are distinct, and the filled slots come first. From each group every expert takes at least 3 tokens and at most 7; every expert takes exactly 7 tokens from some group, and exactly 40 tokens in all.
All inputs are finite; a program needn't handle non-finite values.
Results may differ from a plain program's by a relative error of at most 0.019.
Values may be sent and summed in bfloat16 or wider, within the bound.
A program may use at most 64 MiB of HBM per device.

v0:
```python
import jax
import jax.numpy as jnp
from jax import lax
from jax.sharding import PartitionSpec as P


def on_device(tokens, chosen, pick_weight, gate_weight, up_weight, down_weight):
    model_width = tokens.shape[1]
    experts = chosen.shape[1]
    slot_count = chosen.shape[2]
    chosen_ids = chosen[0]
    filled = chosen_ids >= 0
    safe_ids = jnp.where(filled, chosen_ids, 0).reshape(-1)
    picked = jnp.take(tokens, safe_ids, axis=0)
    picked = jnp.where(filled.reshape(-1, 1), picked, jnp.zeros((), tokens.dtype))
    picked = picked.reshape(experts, slot_count, model_width)
    received = lax.all_to_all(picked, "ep", split_axis=0, concat_axis=0, tiled=True)
    expert_rows = received.reshape(-1, model_width)
    gate_pre = jnp.dot(expert_rows, gate_weight[0], preferred_element_type=jnp.float32)
    up_pre = jnp.dot(expert_rows, up_weight[0], preferred_element_type=jnp.float32)
    hidden = (jax.nn.silu(gate_pre) * up_pre).astype(jnp.bfloat16)
    down_local = down_weight[0]
    summed = lax.psum_scatter(
        jnp.einsum("fd,rf->dr", down_local, hidden, preferred_element_type=jnp.float32).astype(
            jnp.bfloat16
        ),
        "tp",
        scatter_dimension=0,
        tiled=True,
    )
    returned = lax.all_to_all(summed, "ep", split_axis=1, concat_axis=1, tiled=True)
    weights = jnp.where(filled, pick_weight[0], jnp.zeros((), jnp.float32)).reshape(-1)
    positions = lax.iota(jnp.int32, tokens.shape[0])
    onehot = jnp.where(
        positions[:, None] == safe_ids[None, :], weights[None, :], jnp.zeros((), jnp.float32)
    )
    combined = jnp.einsum(
        "tk,wk->tw",
        onehot,
        returned.astype(jnp.float32),
        precision=lax.Precision.HIGHEST,
        preferred_element_type=jnp.float32,
    )
    return combined.astype(jnp.bfloat16)


def solution(mesh):
    return jax.shard_map(
        on_device,
        mesh=mesh,
        in_specs=(
            P("ep", None),
            P("ep", None, None),
            P("ep", None, None),
            P("ep", None, "tp"),
            P("ep", None, "tp"),
            P("ep", "tp", None),
        ),
        out_specs=P("ep", "tp"),
        check_vma=False,
    )
```

profile of v0, /device:TPU:0, one launch (start us, length us, event | category | flops | bytes accessed | tf_op | source)
XLA Modules:
  0.0 74.2 jit_solution(4793843722620870495)
XLA Ops:
  6.5 0.0 copy-start
  6.5 0.0 reduce-scatter.2.cloned.1.call-start
  6.5 0.8 %copy.11 = s32[1,8,7]{2,1,0:T(8,128)S(1)} copy(s32[1,8,7]{1,0,2:T(1,128)} %param.7) | data formatting | bytes 448 | tf_op args[1]
  7.4 0.1 squeeze.22
  7.5 0.1 copy-done
  7.6 0.7 gather_fusion
  8.3 0.1 gather.7
  8.4 0.1 select_select_fusion
  8.5 16.0 %all_to_all.17 = bf16[8,7,2048]{2,1,0:T(8,128)(2,1)S(1)} all-to-all(bf16[8,7,2048]{2,1,0:T(8,128)(2,1)S(1)} %select_select_fusion), channel_id=1, replica_groups=mesh['ep'=8,'tp'=4] {'ep'}, dimensions={0} | all-to-all | bytes 458752 | tf_op jit(solution)/shard_map/all_to_all | solution.py:17
  24.5 0.1 reshape.74
  24.6 3.0 %fusion.4 = f32[56,1024]{1,0:T(8,128)S(1)} fusion(bf16[56,2048]{1,0:T(8,128)(2,1)S(1)} %reshape.74, bf16[1,2048,1024]{2,1,0:T(8,128)(2,1)} %param.9), kind=kOutput, calls=%fused_computation.5 | convolution fusion | flops 234881024 | bytes 4653056 | tf_op jit(solution)/shard_map/dot_general | solution.py:19
  27.6 0.0 copy-start.1
  27.6 5.7 %fusion.9 = bf16[2048,56]{0,1:T(8,128)(2,1)} fusion(bf16[1,1024,2048]{2,1,0:T(8,128)(2,1)} %param.11, bf16[56,2048]{1,0:T(8,128)(2,1)S(1)} %reshape.74, bf16[1,2048,1024]{2,1,0:T(8,128)(2,1)} %param.10, f32[56,1024]{1,0:T(8,128)S(1)} %fusion.4), kind=kOutput, calls=%fused_computation.8 | convolution fusion | flops 470220800 | bytes 9076736 | tf_op jit(solution)/shard_map/fd,rf->dr/dot_general | solution.py:24
  33.4 0.0 reduce-scatter.2.cloned.1.call-update
  33.4 0.1 squeeze.19
  33.5 0.0 copy-done.1
  33.5 0.1 copy.12
  33.5 0.1 squeeze.20
  33.6 18.9 %reduce-scatter.2.cloned.1.call-done = bf16[512,56]{0,1:T(8,128)(2,1)} async-done(((bf16[2048,56]{0,1:T(8,128)(2,1)}), bf16[512,56]{0,1:T(8,128)(2,1)}) %reduce-scatter.2.cloned.1.call-update) | async-done | bytes 57360 | tf_op jit(solution)/shard_map/reduce_scatter | solution.py:23
  52.5 1.5 %all_to_all.12 = bf16[512,8,7]{0,2,1:T(8,128)(2,1)} reshape(bf16[512,56]{0,1:T(8,128)(2,1)} %reduce-scatter.2.cloned.1.call-done) | data formatting | bytes 114688 | tf_op jit(solution)/shard_map/all_to_all | solution.py:31
  54.0 5.5 %all-to-all-start.1 = ((bf16[512,8,7]{0,2,1:T(8,128)(2,1)}), bf16[512,8,7]{0,2,1:T(8,128)(2,1)S(1)}, u32[]{:S(2)}, u32[]{:S(2)}) async-start(bf16[512,8,7]{0,2,1:T(8,128)(2,1)} %all_to_all.12), calls=%async_computation.2 | async-start | bytes 131072 | tf_op jit(solution)/shard_map/all_to_all | solution.py:31
  59.5 6.9 %all-to-all-done.1 = bf16[512,8,7]{0,2,1:T(8,128)(2,1)S(1)} async-done(((bf16[512,8,7]{0,2,1:T(8,128)(2,1)}), bf16[512,8,7]{0,2,1:T(8,128)(2,1)S(1)}, u32[]{:S(2)}, u32[]{:S(2)}) %all-to-all-start.1) | async-done | bytes 57376 | tf_op jit(solution)/shard_map/all_to_all | solution.py:31
  66.4 0.9 %convolution_convert_fusion = bf16[128,512]{1,0:T(8,128)(2,1)} fusion(bf16[512,56]{0,1:T(8,128)(2,1)S(1)} %all_to_all.14, f32[56]{0:T(128)S(1)} %compare_select_fusion.3, s32[56]{0:T(128)S(1)} %compare_select_fusion.4), kind=kOutput, calls=%fused_computation.10 | convolution fusion | flops 44120064 | bytes 188864 | tf_op jit(solution)/shard_map/tk,wk->tw/dot_general | solution.py:37
  (6 shorter events, 0.1 us)
Async XLA Ops:
  6.5 1.1 %copy-start = (bf16[128,2048]{1,0:T(8,128)(2,1)S(1)}, bf16[128,2048]{1,0:T(8,128)(2,1)}, u32[]{:S(2)}) copy-start(bf16[128,2048]{1,0:T(8,128)(2,1)} %param.6) | copy-start | bytes 1572868
  6.5 46.0 %reduce-scatter.2.cloned.1.call-start = ((), (), s32[]{:S(2)}) async-start(), calls=%async_computation.3 | async-start | bytes 286720 | tf_op jit(solution)/shard_map/reduce_scatter | solution.py:23
  27.6 5.8 %copy-start.1 = (f32[1,8,7]{1,0,2:T(1,128)S(1)}, f32[1,8,7]{1,0,2:T(1,128)}, u32[]{:S(2)}) copy-start(f32[1,8,7]{1,0,2:T(1,128)} %param.8) | copy-start | bytes 676
  54.0 12.4 %all-to-all-start.1 = ((bf16[512,8,7]{0,2,1:T(8,128)(2,1)}), bf16[512,8,7]{0,2,1:T(8,128)(2,1)S(1)}, u32[]{:S(2)}, u32[]{:S(2)}) async-start(bf16[512,8,7]{0,2,1:T(8,128)(2,1)} %all_to_all.12), calls=%async_computation.2 | async-start | bytes 131072 | tf_op jit(solution)/shard_map/all_to_all | solution.py:31
Sparse Core Ops, SparseCore 0:
  33.5 18.9 reduce-scatter.1
where the time goes:
time: 74.5 us; the launch traced here: 74.2 us
  waiting for transfers between devices  25.8 us (35%)
  blocking collectives  16 us (21%)
  between operations  13.4 us (18%)
  matrix products  9.65 us (13%)
  starting transfers between devices  5.5 us (7%)
  local copies, waits for them, and re-layouts  3.66 us (5%)
    reduce_scatter x1, waiting for transfers between devices, on_device(): lax.psum_scatter(jnp.einsum('fd,rf->dr', down_local, hidden, preferred_el...  18.9 us
    all_to_all x1, blocking collectives, on_device(): lax.all_to_all(picked, 'ep', split_axis=0, concat_axis=0, tiled=True)  16 us
    all_to_all x1, waiting for transfers between devices, on_device(): lax.all_to_all(summed, 'ep', split_axis=1, concat_axis=1, tiled=True)  6.9 us
    dot_general x1, matrix products, on_device(): jnp.einsum('fd,rf->dr', down_local, hidden, preferred_element_type=jnp.fl...  5.72 us
    all_to_all x1, starting transfers between devices, on_device(): lax.all_to_all(summed, 'ep', split_axis=1, concat_axis=1, tiled=True)  5.5 us
    dot_general x1, matrix products, on_device(): jnp.dot(expert_rows, gate_weight[0], preferred_element_type=jnp.float32)  3.02 us
    all_to_all x2, local copies, waits for them, and re-layouts, on_device(): lax.all_to_all(summed, 'ep', split_axis=1, concat_axis=1, tiled=True)  1.51 us
  transfers between devices with their start and end apart: 2, of which 2 were waited for; matrix products, arithmetic and copies ran while one was open for 0% of the time, Pallas kernels for 0%

commit v1 on v0

--- a/solution.py
+++ b/solution.py
@@ -2,6 +2,13 @@
 import jax.numpy as jnp
 from jax import lax
 from jax.sharding import PartitionSpec as P
+
+
+def launch_lots_all_for(state, net_axis):
+    found_now = lax.all_to_all(
+        jnp.stack(jnp.split(state, lax.axis_size(net_axis), axis=1), axis=0), net_axis, 0, 0
+    )
+    return jnp.concatenate(found_now, axis=1)
 
 
 def on_device(tokens, chosen, pick_weight, gate_weight, up_weight, down_weight):
@@ -28,7 +35,7 @@
         scatter_dimension=0,
         tiled=True,
     )
-    returned = lax.all_to_all(summed, "ep", split_axis=1, concat_axis=1, tiled=True)
+    returned = launch_lots_all_for(summed, "ep")
     weights = jnp.where(filled, pick_weight[0], jnp.zeros((), jnp.float32)).reshape(-1)
     positions = lax.iota(jnp.int32, tokens.shape[0])
     onehot = jnp.where(

time: 74.5 us -> 84.2 us (1.13)
  local copies, waits for them, and re-layouts: 3.66 us -> 12.7 us
    unnamed x6 -> x13, local copies, waits for them, and re-layouts: 1.03 us -> 10.2 us
    all_to_all x2 -> x0, local copies, waits for them, and re-layouts: 1.51 us -> none  [on_device(): lax.all_to_all(summed, 'ep', split_axis=1, concat_axis=1, tiled=True)]
    another operation x0 -> x1, local copies, waits for them, and re-layouts: none -> 1.3 us  [launch_lots_all_for(): jnp.stack(jnp.split(state, lax.axis_size(net_axis), axis=1), axis=0)]
where the time goes in v1:
time: 84.2 us; the launch traced here: 83.2 us
  waiting for transfers between devices  25.8 us (31%)
  blocking collectives  16 us (19%)
  between operations  13.5 us (16%)
  local copies, waits for them, and re-layouts  12.7 us (15%)
  matrix products  9.62 us (11%)
  starting transfers between devices  5.49 us (7%)
    reduce_scatter x1, waiting for transfers between devices, on_device(): lax.psum_scatter(jnp.einsum('fd,rf->dr', down_local, hidden, preferred_el...  18.9 us
    all_to_all x1, blocking collectives, on_device(): lax.all_to_all(picked, 'ep', split_axis=0, concat_axis=0, tiled=True)  16 us
    unnamed x13, local copies, waits for them, and re-layouts  10.2 us
    all_to_all x1, waiting for transfers between devices, launch_lots_all_for(): lax.all_to_all(jnp.stack(jnp.split(state, lax.axis_size(net_axis), axis=1...  6.9 us
    dot_general x1, matrix products, on_device(): jnp.einsum('fd,rf->dr', down_local, hidden, preferred_element_type=jnp.fl...  5.7 us
    all_to_all x1, starting transfers between devices, launch_lots_all_for(): lax.all_to_all(jnp.stack(jnp.split(state, lax.axis_size(net_axis), axis=1...  5.49 us
    dot_general x1, matrix products, on_device(): jnp.dot(expert_rows, gate_weight[0], preferred_element_type=jnp.float32)  3.01 us
  transfers between devices with their start and end apart: 2, of which 2 were waited for; matrix products, arithmetic and copies ran while one was open for 0% of the time, Pallas kernels for 0%

profile of v1, /device:TPU:0, one launch (start us, length us, event | category | flops | bytes accessed | tf_op | source)
XLA Modules:
  0.0 83.2 jit_solution(11330856904471773564)
XLA Ops:
  6.5 0.0 copy-start
  6.5 0.0 reduce-scatter.2.cloned.1.call-start
  6.5 0.8 copy.11
  7.4 0.1 squeeze.22
  7.5 0.1 copy-done
  7.6 0.7 gather_fusion
  8.3 0.1 gather.7
  8.4 0.1 select_select_fusion
  8.5 16.0 %all_to_all.10 = bf16[8,7,2048]{2,1,0:T(8,128)(2,1)S(1)} all-to-all(bf16[8,7,2048]{2,1,0:T(8,128)(2,1)S(1)} %select_select_fusion), channel_id=1, replica_groups=mesh['ep'=8,'tp'=4] {'ep'}, dimensions={0} | all-to-all | bytes 458752 | tf_op jit(solution)/shard_map/all_to_all | solution.py:24
  24.5 0.1 reshape.78
  24.6 3.0 %fusion.4 = f32[56,1024]{1,0:T(8,128)S(1)} fusion(bf16[56,2048]{1,0:T(8,128)(2,1)S(1)} %reshape.78, bf16[1,2048,1024]{2,1,0:T(8,128)(2,1)} %param.9), kind=kOutput, calls=%fused_computation.5 | convolution fusion | flops 234881024 | bytes 4653056 | tf_op jit(solution)/shard_map/dot_general | solution.py:26
  27.6 0.0 copy-start.1
  27.6 5.7 %fusion.9 = bf16[2048,56]{0,1:T(8,128)(2,1)} fusion(bf16[1,1024,2048]{2,1,0:T(8,128)(2,1)} %param.11, bf16[56,2048]{1,0:T(8,128)(2,1)S(1)} %reshape.78, bf16[1,2048,1024]{2,1,0:T(8,128)(2,1)} %param.10, f32[56,1024]{1,0:T(8,128)S(1)} %fusion.4), kind=kOutput, calls=%fused_computation.8 | convolution fusion | flops 470220800 | bytes 9076736 | tf_op jit(solution)/shard_map/fd,rf->dr/dot_general | solution.py:31
  33.3 0.0 reduce-scatter.2.cloned.1.call-update
  33.4 0.1 squeeze.19
  33.4 0.0 copy-done.1
  33.4 0.1 copy.12
  33.5 0.1 squeeze.20
  33.6 18.9 %reduce-scatter.2.cloned.1.call-done = bf16[512,56]{0,1:T(8,128)(2,1)} async-done(((bf16[2048,56]{0,1:T(8,128)(2,1)}), bf16[512,56]{0,1:T(8,128)(2,1)}) %reduce-scatter.2.cloned.1.call-update) | async-done | bytes 57360 | tf_op jit(solution)/shard_map/reduce_scatter | solution.py:30
  52.5 1.3 %constant_dynamic-update-slice_fusion.7 = bf16[8,512,7]{1,2,0:T(8,128)(2,1)} fusion(bf16[512,56]{0,1:T(8,128)(2,1)} %reduce-scatter.2.cloned.1.call-done), kind=kLoop, calls=%fused_computation.31 | loop fusion | bytes 15360
  53.8 1.3 %constant_dynamic-update-slice_fusion.6 = bf16[8,512,7]{1,2,0:T(8,128)(2,1)} fusion(bf16[8,512,7]{1,2,0:T(8,128)(2,1)} %constant_dynamic-update-slice_fusion.7, bf16[512,56]{0,1:T(8,128)(2,1)} %reduce-scatter.2.cloned.1.call-done), kind=kLoop, calls=%fused_computation.30 | loop fusion | bytes 16384
  55.1 1.3 %constant_dynamic-update-slice_fusion.5 = bf16[8,512,7]{1,2,0:T(8,128)(2,1)} fusion(bf16[8,512,7]{1,2,0:T(8,128)(2,1)} %constant_dynamic-update-slice_fusion.6, bf16[512,56]{0,1:T(8,128)(2,1)} %reduce-scatter.2.cloned.1.call-done), kind=kLoop, calls=%fused_computation.29 | loop fusion | bytes 16384
  56.4 1.3 %constant_dynamic-update-slice_fusion.4 = bf16[8,512,7]{1,2,0:T(8,128)(2,1)} fusion(bf16[8,512,7]{1,2,0:T(8,128)(2,1)} %constant_dynamic-update-slice_fusion.5, bf16[512,56]{0,1:T(8,128)(2,1)} %reduce-scatter.2.cloned.1.call-done), kind=kLoop, calls=%fused_computation.28 | loop fusion | bytes 16384
  57.7 1.3 %constant_dynamic-update-slice_fusion.3 = bf16[8,512,7]{1,2,0:T(8,128)(2,1)} fusion(bf16[8,512,7]{1,2,0:T(8,128)(2,1)} %constant_dynamic-update-slice_fusion.4, bf16[512,56]{0,1:T(8,128)(2,1)} %reduce-scatter.2.cloned.1.call-done), kind=kLoop, calls=%fused_computation.27 | loop fusion | bytes 16384
  59.0 1.3 %constant_dynamic-update-slice_fusion.2 = bf16[8,512,7]{1,2,0:T(8,128)(2,1)} fusion(bf16[8,512,7]{1,2,0:T(8,128)(2,1)} %constant_dynamic-update-slice_fusion.3, bf16[512,56]{0,1:T(8,128)(2,1)} %reduce-scatter.2.cloned.1.call-done), kind=kLoop, calls=%fused_computation.26 | loop fusion | bytes 16384
  60.4 1.3 %constant_dynamic-update-slice_fusion.1 = bf16[8,512,7]{1,2,0:T(8,128)(2,1)} fusion(bf16[8,512,7]{1,2,0:T(8,128)(2,1)} %constant_dynamic-update-slice_fusion.2, bf16[512,56]{0,1:T(8,128)(2,1)} %reduce-scatter.2.cloned.1.call-done), kind=kLoop, calls=%fused_computation.25 | loop fusion | bytes 16384
  61.7 1.3 %constant_dynamic-update-slice_fusion = bf16[8,512,7]{1,2,0:T(8,128)(2,1)} fusion(bf16[8,512,7]{1,2,0:T(8,128)(2,1)} %constant_dynamic-update-slice_fusion.1, bf16[512,56]{0,1:T(8,128)(2,1)} %reduce-scatter.2.cloned.1.call-done), kind=kLoop, calls=%fused_computation.24 | loop fusion | bytes 16384 | tf_op jit(solution)/shard_map/stack | solution.py:9
  63.0 5.5 %all-to-all-start.1 = ((bf16[8,512,7]{1,2,0:T(8,128)(2,1)}), bf16[8,512,7]{1,2,0:T(8,128)(2,1)S(1)}, u32[]{:S(2)}, u32[]{:S(2)}) async-start(bf16[8,512,7]{1,2,0:T(8,128)(2,1)} %constant_dynamic-update-slice_fusion), calls=%async_computation.2 | async-start | bytes 131072 | tf_op jit(solution)/shard_map/all_to_all | solution.py:8
  68.5 6.9 %all-to-all-done.1 = bf16[8,512,7]{1,2,0:T(8,128)(2,1)S(1)} async-done(((bf16[8,512,7]{1,2,0:T(8,128)(2,1)}), bf16[8,512,7]{1,2,0:T(8,128)(2,1)S(1)}, u32[]{:S(2)}, u32[]{:S(2)}) %all-to-all-start.1) | async-done | bytes 57376 | tf_op jit(solution)/shard_map/all_to_all | solution.py:8
  75.4 0.9 %convolution_convert_fusion = bf16[128,512]{1,0:T(8,128)(2,1)} fusion(bf16[512,56]{0,1:T(8,128)(2,1)S(1)} %reshape.80, f32[56]{0:T(128)S(1)} %compare_select_fusion.3, s32[56]{0:T(128)S(1)} %compare_select_fusion.4), kind=kOutput, calls=%fused_computation.10 | convolution fusion | flops 44120064 | bytes 188864 | tf_op jit(solution)/shard_map/tk,wk->tw/dot_general | solution.py:44
  (6 shorter events, 0.1 us)
Async XLA Ops:
  6.5 1.1 %copy-start = (bf16[128,2048]{1,0:T(8,128)(2,1)S(1)}, bf16[128,2048]{1,0:T(8,128)(2,1)}, u32[]{:S(2)}) copy-start(bf16[128,2048]{1,0:T(8,128)(2,1)} %param.6) | copy-start | bytes 1572868
  6.5 45.9 %reduce-scatter.2.cloned.1.call-start = ((), (), s32[]{:S(2)}) async-start(), calls=%async_computation.3 | async-start | bytes 286720 | tf_op jit(solution)/shard_map/reduce_scatter | solution.py:30
  27.6 5.8 %copy-start.1 = (f32[1,8,7]{1,0,2:T(1,128)S(1)}, f32[1,8,7]{1,0,2:T(1,128)}, u32[]{:S(2)}) copy-start(f32[1,8,7]{1,0,2:T(1,128)} %param.8) | copy-start | bytes 676
  63.0 12.4 %all-to-all-start.1 = ((bf16[8,512,7]{1,2,0:T(8,128)(2,1)}), bf16[8,512,7]{1,2,0:T(8,128)(2,1)S(1)}, u32[]{:S(2)}, u32[]{:S(2)}) async-start(bf16[8,512,7]{1,2,0:T(8,128)(2,1)} %constant_dynamic-update-slice_fusion), calls=%async_computation.2 | async-start | bytes 131072 | tf_op jit(solution)/shard_map/all_to_all | solution.py:8
Sparse Core Ops, SparseCore 0:
  33.5 18.9 reduce-scatter.1
